TPU v7x, 512 devices: a 8x2x16 block of a 8x8x16 slice. The times are simulated.
512 devices in a mesh: grp: 2 (over y), sp: 32 (over z, core), tp: 8 (over x).
Axes of the slice: x: 8, y: 2, z: 16, core: 2. Of those that a mesh axis runs over, the one named last changes fastest.
The devices are a block of a 8x8x16 slice.
Arguments:
- out_gate: bfloat16 [24576, 1024], P(('grp', 'sp'), 'tp'), parts along dimension 0, may hold values from -6 to 6
- in_gate: bfloat16 [24576, 1024], P(('grp', 'sp'), 'tp'), parts along dimension 0, may hold values from -6 to 6
- conv_input: bfloat16 [24576, 1024], P(('grp', 'sp'), 'tp'), parts along dimension 0, may hold values from -6 to 6
- doc_ids: int32 [24576], P(('grp', 'sp')), parts along dimension 0, may hold values from 0 to 15, never falling along the last dimension, each value on 1 to 1536 neighbouring positions
- residual: bfloat16 [24576, 2048], P(('grp', 'sp'), 'tp'), parts along dimension 0, may hold values from -6 to 6
- conv_taps: float32 [3, 1024], P(None, 'tp'), may hold values from -6 to 6
- mix_gain: float32 [1024], P('tp'), may hold values from 0.1 to 1.9
- out_weight: bfloat16 [1024, 2048], P('tp'), may hold values from -0.1875 to 0.1875
- ffn_gain: float32 [2048], P('tp'), may hold values from 0.1 to 1.9
- routing: int32 [24576, 2], P(('grp', 'sp')), parts along dimension 0, may hold values from 0 to 63, as said below
- route_weight: float32 [24576, 2], P(('grp', 'sp')), parts along dimension 0, may hold values from 0.2 to 1.2
- expert_gate: bfloat16 [64, 2048, 512], P('sp', None, 'tp'), may hold values from -0.125 to 0.125
- expert_up: bfloat16 [64, 2048, 512], P('sp', None, 'tp'), may hold values from -0.125 to 0.125
- expert_down: bfloat16 [64, 512, 2048], P('sp', None, 'tp'), may hold values from -0.25 to 0.25
- shared_gate: bfloat16 [2048, 512], P(None, 'tp'), may hold values from -0.125 to 0.125
- shared_up: bfloat16 [2048, 512], P(None, 'tp'), may hold values from -0.125 to 0.125
- shared_down: bfloat16 [512, 2048], P(None, 'tp'), may hold values from -0.25 to 0.25
Outputs:
- layer_out: bfloat16 [24576, 2048], P(('grp', 'sp'), 'tp'), parts along dimension 0
There are 2 independent parts, one for each index of `grp`. A program takes and returns all parts, laid end to end along the dimension named above; an argument that names none is the same for every part. Nothing has to cross between parts.
Inputs may be any that keep to these rules, and one draw needn't show every extreme that they name: `routing`: each row names 2 different experts. In each aligned block of 48 rows no expert is named by more than 3 rows, and some expert is named by exactly 3 rows. `doc_ids`: never falls along the sequence; a document holds at most 1536 positions.
All inputs are finite; a program needn't handle non-finite values.
Results may differ from a plain program's by a relative error of at most 0.017.
Values may be sent and summed in bfloat16 or wider, within the bound.
No kernel may reach another device: no remote copies, remote signals or barrier semaphores. Data moves between devices by JAX's collectives and lax.ppermute only.
A program may use at most 64 MiB of HBM per device.

v0:
```python
import jax
import jax.numpy as jnp
from jax import lax
from jax.sharding import PartitionSpec as P

D_CONV = 1024
CONV_K = 3
TOPK = 2
EXP_DEV = 2


def from_behind(value, axis, steps):
    count = lax.axis_size(axis)
    first, last = (max(0, -steps), min(count, count - steps))
    return lax.ppermute(value, axis, [(source, source + steps) for source in range(first, last)])


def sent_to_all(shard, axis):
    copies = jnp.broadcast_to(shard, (lax.axis_size(axis), *shard.shape))
    return lax.all_to_all(copies, axis, split_axis=0, concat_axis=0, tiled=True)


def of_everyone(shard, axis):
    return sent_to_all(shard, axis).sum(axis=0)


def cut_along(shard, dim, length):
    shape = shard.shape
    pieces = shard.reshape(*shape[:dim], length, shape[dim] // length, *shape[dim + 1 :])
    return jnp.moveaxis(pieces, dim, 0)


def sum_at_owner(shard, axis, dim):
    pieces = cut_along(shard, dim, lax.axis_size(axis))
    arrived = lax.all_to_all(pieces, axis, split_axis=0, concat_axis=0, tiled=True)
    return arrived.astype(jnp.float32).sum(axis=0)


def rows_first(arrays, axis, dims):
    turned = [jnp.moveaxis(a, dim, 0) for a, dim in zip(arrays, dims)]
    both = jnp.concatenate([t.reshape(len(t), -1) for t in turned], axis=1)
    whole, at, finished = (lax.all_gather(both, axis, axis=0, tiled=True), 0, [])
    for t, dim in zip(turned, dims):
        slab = whole[:, at : at + t[0].size].reshape(-1, *t.shape[1:])
        finished.append(jnp.moveaxis(slab, 0, dim))
        at += t[0].size
    return tuple(finished)


def body(
    out_gate,
    in_gate,
    conv_input,
    doc_ids,
    residual,
    conv_taps,
    mix_gain,
    out_weight,
    ffn_gain,
    routing,
    route_weight,
    expert_gate,
    expert_up,
    expert_down,
    shared_gate,
    shared_up,
    shared_down,
):
    tokens = residual.shape[0]
    width = out_weight.shape[1]
    n_tp = lax.axis_size("tp")
    n_sp = lax.axis_size("sp")
    rows = tokens // n_tp
    experts = n_sp * EXP_DEV
    most = max(1, 2 * rows * TOPK // experts)
    slots = n_tp * most
    total = experts * slots
    cols = expert_down.shape[2]
    product = (in_gate.astype(jnp.float32) * conv_input.astype(jnp.float32)).astype(jnp.bfloat16)
    tail = (product[tokens - CONV_K + 1 :], doc_ids[tokens - CONV_K + 1 :].astype(jnp.bfloat16))
    prev_rows, prev_docs = from_behind((tail[0], tail[1]), "sp", 1)
    extended = jnp.concatenate([prev_rows, product], axis=0).astype(jnp.float32)
    ext_docs = jnp.concatenate([prev_docs.astype(jnp.int32), doc_ids])
    mixed = jnp.zeros(product.shape, jnp.float32)
    for k in range(CONV_K):
        keep = (ext_docs[k : k + tokens] == doc_ids)[:, None]
        mixed = mixed + jnp.where(keep, conv_taps[k] * extended[k : k + tokens], jnp.float32(0.0))
    conv_out = out_gate.astype(jnp.float32) * mixed
    squares = of_everyone(jnp.sum(conv_out * conv_out, axis=1), "tp")
    normed = (conv_out * lax.rsqrt(squares / D_CONV + 1e-06)[:, None] * mix_gain).astype(
        jnp.bfloat16
    )
    partial_value = jnp.dot(normed, out_weight, preferred_element_type=jnp.float32)
    proj = sum_at_owner(partial_value.astype(jnp.bfloat16), "tp", 1)
    stream = (residual.astype(jnp.float32) + proj).astype(jnp.bfloat16)
    stream32 = stream.astype(jnp.float32)
    stream_sq = of_everyone(jnp.sum(stream32 * stream32, axis=1), "tp")
    normal_cols = (stream32 * lax.rsqrt(stream_sq / width + 1e-06)[:, None] * ffn_gain).astype(
        jnp.bfloat16
    )
    flat_expert = routing.reshape(-1)
    onehot = (flat_expert[:, None] == jnp.arange(experts, dtype=jnp.int32)[None, :]).astype(
        jnp.int32
    )
    blocked = onehot.reshape(n_tp, rows * TOPK, experts)
    earlier = jnp.cumsum(blocked, axis=1) - blocked
    position = jnp.sum(earlier * blocked, axis=2).reshape(-1)
    entry = jnp.arange(tokens * TOPK, dtype=jnp.int32)
    slot = flat_expert * slots + entry // (rows * TOPK) * most + position
    table = jnp.full((total,), tokens, jnp.int32).at[slot].set(entry // TOPK)
    block_rows = lax.all_to_all(normal_cols, "tp", split_axis=0, concat_axis=1, tiled=True)
    mine = lax.dynamic_index_in_dim(
        table.reshape(n_sp, EXP_DEV, n_tp, most), lax.axis_index("tp"), 2, False
    )
    local = jnp.where(mine >= tokens, rows, mine - lax.axis_index("tp") * rows)
    padded_block = jnp.concatenate([block_rows, jnp.zeros((1, width), jnp.bfloat16)], axis=0)
    got = lax.all_to_all(padded_block[local], "sp", split_axis=0, concat_axis=0, tiled=True)
    arrived, whole = (
        lax.all_gather(got, "tp", axis=2, tiled=True),
        lax.all_gather(block_rows.reshape(1, 1, rows, width), "tp", axis=2, tiled=True),
    )
    normal = whole.reshape(tokens, width)
    gate = jnp.einsum("nesd,edh->nesh", arrived, expert_gate, preferred_element_type=jnp.float32)
    upper = jnp.einsum("nesd,edh->nesh", arrived, expert_up, preferred_element_type=jnp.float32)
    hidden = (jax.nn.silu(gate) * upper).astype(jnp.bfloat16)
    hidden_flat = hidden.reshape(n_sp * EXP_DEV * slots, hidden.shape[3])
    shared_hid = (
        jax.nn.silu(jnp.dot(normal, shared_gate, preferred_element_type=jnp.float32))
        * jnp.dot(normal, shared_up, preferred_element_type=jnp.float32)
    ).astype(jnp.bfloat16)
    expert_piece, shared_piece = rows_first((hidden_flat, shared_hid), "tp", (1, 1))
    count = expert_piece.shape[1]
    expert_part = jnp.einsum(
        "nesh,ehd->nesd",
        expert_piece.reshape(n_sp, EXP_DEV, slots, count),
        expert_down,
        preferred_element_type=jnp.float32,
    )
    shared_part = jnp.dot(shared_piece, shared_down, preferred_element_type=jnp.float32)
    returned = lax.all_to_all(
        expert_part.astype(jnp.bfloat16), "sp", split_axis=0, concat_axis=0, tiled=True
    )
    picked = (
        returned.reshape(total, cols)[slot].astype(jnp.float32) * route_weight.reshape(-1)[:, None]
    )
    routed = jnp.sum(picked.reshape(tokens, TOPK, cols), axis=1)
    return (stream32 + shared_part + routed).astype(jnp.bfloat16)


def solution(mesh):
    return jax.shard_map(
        body,
        mesh=mesh,
        in_specs=(
            P(("grp", "sp"), "tp"),
            P(("grp", "sp"), "tp"),
            P(("grp", "sp"), "tp"),
            P(("grp", "sp")),
            P(("grp", "sp"), "tp"),
            P(None, "tp"),
            P("tp"),
            P("tp", None),
            P("tp"),
            P(("grp", "sp"), None),
            P(("grp", "sp"), None),
            P("sp", None, "tp"),
            P("sp", None, "tp"),
            P("sp", None, "tp"),
            P(None, "tp"),
            P(None, "tp"),
            P(None, "tp"),
        ),
        out_specs=P(("grp", "sp"), "tp"),
        check_vma=False,
    )
```

profile of v0, /device:TPU:65, one launch (start us, length us, event | category | flops | bytes accessed | tf_op | source)
XLA Modules:
  0.0 412.4 jit_solution(5063214200456433942)
XLA Ops:
  7.6 7.1 %collective-permute-start.1 = (bf16[2,128]{1,0:T(2,128)(2,1)S(1)}, bf16[2,128]{1,0:T(2,128)(2,1)S(1)}, u32[]{:S(2)}, u32[]{:S(2)}) collective-permute-start(bf16[2,128]{1,0:T(2,128)(2,1)S(1)} %slice.53), channel_id=1, source_target_pairs={{0,8},{8,16},{16,24},{24,32},{32,40},{40,48},{48,56},{56,64},{64,7... | collective-permute-start | bytes 1544 | tf_op jit(solution)/shard_map/ppermute | solution.py:15
  15.4 1.9 collective-permute-start
  18.2 34.9 %collective-permute-done = bf16[2]{0:T(256)(128)(2,1)S(1)} collective-permute-done((bf16[2]{0:T(256)(128)(2,1)S(1)}, bf16[2]{0:T(256)(128)(2,1)S(1)}, u32[]{:S(2)}, u32[]{:S(2)}) %collective-permute-start) | collective-permute-done | bytes 36 | tf_op jit(solution)/shard_map/ppermute | solution.py:15
  55.8 9.1 %all_to_all.46 = f32[8,1,384]{2,1,0:T(1,128)S(1)} all-to-all(f32[8,1,384]{2,1,0:T(1,128)S(1)} %broadcast_in_dim.50), channel_id=1, replica_groups=mesh['grp'=2,'sp'=32,'tp'=8] {'tp'}, dimensions={0} | all-to-all | bytes 24576 | tf_op jit(solution)/shard_map/all_to_all | solution.py:20
  65.5 1.3 copy.114
  66.8 3.9 all-to-all-start.1
  71.1 1.9 select_reduce_fusion
  73.5 35.1 %all-to-all-done.1 = bf16[8,384,256]{2,1,0:T(8,128)(2,1)S(1)} async-done(((bf16[8,384,256]{2,1,0:T(8,128)(2,1)}), bf16[8,384,256]{2,1,0:T(8,128)(2,1)S(1)}, u32[]{:S(2)}, u32[]{:S(2)}) %all-to-all-start.1) | async-done | bytes 1572896 | tf_op jit(solution)/shard_map/all_to_all | solution.py:35
  109.6 3.7 all-to-all-start.2
  113.3 3.4 scatter_custom_fusion
  116.9 3.0 all-to-all-done.2
  120.8 3.7 all-to-all-start.3
  124.7 8.5 %all-to-all-done.3 = bf16[8,48,256]{2,1,0:T(8,128)(2,1)S(1)} async-done(((bf16[8,48,256]{2,1,0:T(8,128)(2,1)}), bf16[8,48,256]{2,1,0:T(8,128)(2,1)S(1)}, u32[]{:S(2)}, u32[]{:S(2)}) %all-to-all-start.3) | async-done | bytes 196640 | tf_op jit(solution)/shard_map/all_to_all | solution.py:111
  134.8 1.9 copy.75
  136.7 15.3 %all-to-all-start.4 = ((bf16[32,2,3,2048]{3,1,2,0:T(2,128)(2,1)}), bf16[32,2,3,2048]{3,1,2,0:T(2,128)(2,1)S(1)}, u32[]{:S(2)}, u32[]{:S(2)}) async-start(bf16[32,2,3,2048]{3,1,2,0:T(2,128)(2,1)} %copy.75), calls=%async_computation.4 | async-start | bytes 1572864 | tf_op jit(solution)/shard_map/all_to_all | solution.py:117
  153.1 43.3 %all-to-all-done.4 = bf16[32,2,3,2048]{3,1,2,0:T(2,128)(2,1)S(1)} async-done(((bf16[32,2,3,2048]{3,1,2,0:T(2,128)(2,1)}), bf16[32,2,3,2048]{3,1,2,0:T(2,128)(2,1)S(1)}, u32[]{:S(2)}, u32[]{:S(2)}) %all-to-all-start.4) | async-done | bytes 786464 | tf_op jit(solution)/shard_map/all_to_all | solution.py:117
  196.4 1.2 copy.76
  198.0 2.1 fusion.30
  200.2 1.6 fusion.39
  201.9 76.6 %all-gather.4.cloned.1.call-done = bf16[32,2,24,2048]{3,0,1,2:T(8,128)(2,1)} async-done(((bf16[32,2,3,2048]{3,0,1,2:T(8,128)(2,1)}), bf16[32,2,24,2048]{3,0,1,2:T(8,128)(2,1)}) %all-gather.4.cloned.1.call-update) | async-done | bytes 6291472 | tf_op jit(solution)/shard_map/all_gather | solution.py:119
  278.6 4.7 %fusion.16 = f32[32,2,24,64]{3,0,2,1:T(8,128)S(1)} fusion(bf16[32,2,24,2048]{3,0,1,2:T(8,128)(2,1)} %all-gather.4.cloned.1.call-done, bf16[2,2048,64]{1,2,0:T(8,128)(2,1)S(1)} %copy-done.10), kind=kOutput, calls=%fused_computation.18 | convolution fusion | flops 402653184 | bytes 7208960 | tf_op jit(solution)/shard_map/nesd,edh->nesh/dot_general | solution.py:123
  283.3 1.8 fusion.25
  286.3 42.3 %all-gather.8.cloned.1.call-done = bf16[512,1920]{1,0:T(8,128)(2,1)} async-done(((bf16[64,1920]{1,0:T(8,128)(2,1)}), bf16[512,1920]{1,0:T(8,128)(2,1)}) %all-gather.8.cloned.1.call-update) | async-done | bytes 1966096 | tf_op jit(solution)/shard_map/all_gather | solution.py:42
  328.7 1.4 slice-done
  330.1 1.6 copy.92
  331.6 2.1 fusion.13
  334.7 18.1 %all-to-all-start.5 = ((bf16[32,2,24,256]{3,2,1,0:T(8,128)(2,1)}), bf16[32,2,24,256]{3,2,1,0:T(8,128)(2,1)S(1)}, u32[]{:S(2)}, u32[]{:S(2)}) async-start(bf16[32,2,24,256]{3,2,1,0:T(8,128)(2,1)} %copy.85), calls=%async_computation.5 | async-start | bytes 1572864 | tf_op jit(solution)/shard_map/all_to_all | solution.py:140
  353.6 43.6 %all-to-all-done.5 = bf16[32,2,24,256]{3,2,1,0:T(8,128)(2,1)S(1)} async-done(((bf16[32,2,24,256]{3,2,1,0:T(8,128)(2,1)}), bf16[32,2,24,256]{3,2,1,0:T(8,128)(2,1)S(1)}, u32[]{:S(2)}, u32[]{:S(2)}) %all-to-all-start.5) | async-done | bytes 786464 | tf_op jit(solution)/shard_map/all_to_all | solution.py:140
  397.2 3.3 gather_fusion.1
  400.4 1.5 reshape.187
  402.0 2.0 multiply_reduce_fusion
  403.9 1.9 fusion.29
  (81 shorter events, 15.2 us)
Async XLA Ops:
  6.5 58.3 %copy-start = (bf16[128,2048]{1,0:T(8,128)(2,1)S(1)}, bf16[128,2048]{1,0:T(8,128)(2,1)}, u32[]{:S(2)}) copy-start(bf16[128,2048]{1,0:T(8,128)(2,1)} %param.24) | copy-start | bytes 1572868
  6.6 58.3 %copy-start.8 = (f32[128]{0:T(128)S(1)}, f32[128]{0:T(128)}, u32[]{:S(2)}) copy-start(f32[128]{0:T(128)} %param.23) | copy-start | bytes 1540
  7.6 47.0 %collective-permute-start.1 = (bf16[2,128]{1,0:T(2,128)(2,1)S(1)}, bf16[2,128]{1,0:T(2,128)(2,1)S(1)}, u32[]{:S(2)}, u32[]{:S(2)}) collective-permute-start(bf16[2,128]{1,0:T(2,128)(2,1)S(1)} %slice.53), channel_id=1, source_target_pairs={{0,8},{8,16},{16,24},{24,32},{32,40},{40,48},{48,56},{56,64},{64,7... | collective-permute-start | bytes 1544 | tf_op jit(solution)/shard_map/ppermute | solution.py:15
  15.4 37.6 %collective-permute-start = (bf16[2]{0:T(256)(128)(2,1)S(1)}, bf16[2]{0:T(256)(128)(2,1)S(1)}, u32[]{:S(2)}, u32[]{:S(2)}) collective-permute-start(bf16[2]{0:T(256)(128)(2,1)S(1)} %slice.37), channel_id=1, source_target_pairs={{0,8},{8,16},{16,24},{24,32},{32,40},{40,48},{48,56},{56,64},{64,7... | collective-permute-start | bytes 20 | tf_op jit(solution)/shard_map/ppermute | solution.py:15
  66.8 3.9 copy-start.5
  66.8 41.9 %all-to-all-start.1 = ((bf16[8,384,256]{2,1,0:T(8,128)(2,1)}), bf16[8,384,256]{2,1,0:T(8,128)(2,1)S(1)}, u32[]{:S(2)}, u32[]{:S(2)}) async-start(bf16[8,384,256]{2,1,0:T(8,128)(2,1)} %bitcast.76), calls=%async_computation.1 | async-start | bytes 3145728 | tf_op jit(solution)/shard_map/all_to_all | solution.py:35
  70.7 38.2 %copy-start.4 = (bf16[384,256]{1,0:T(8,128)(2,1)S(1)}, bf16[384,256]{1,0:T(8,128)(2,1)}, u32[]{:S(2)}) copy-start(bf16[384,256]{1,0:T(8,128)(2,1)} %param.21) | copy-start | bytes 589828
  73.5 46.5 %copy-start.7 = (f32[256]{0:T(256)S(1)}, f32[256]{0:T(256)}, u32[]{:S(2)}) copy-start(f32[256]{0:T(256)} %param.25) | copy-start | bytes 3076
  109.6 10.3 %all-to-all-start.2 = ((f32[8,1,384]{2,1,0:T(1,128)}), f32[8,1,384]{2,1,0:T(1,128)S(1)}, u32[]{:S(2)}, u32[]{:S(2)}) async-start(f32[8,1,384]{2,1,0:T(1,128)} %broadcast_in_dim.51), calls=%async_computation.2 | async-start | bytes 24576 | tf_op jit(solution)/shard_map/all_to_all | solution.py:20
  120.8 12.4 %all-to-all-start.3 = ((bf16[8,48,256]{2,1,0:T(8,128)(2,1)}), bf16[8,48,256]{2,1,0:T(8,128)(2,1)S(1)}, u32[]{:S(2)}, u32[]{:S(2)}) async-start(bf16[8,48,256]{2,1,0:T(8,128)(2,1)} %bitcast.4), calls=%async_computation.3 | async-start | bytes 393216 | tf_op jit(solution)/shard_map/all_to_all | solution.py:111
  136.7 59.7 %all-to-all-start.4 = ((bf16[32,2,3,2048]{3,1,2,0:T(2,128)(2,1)}), bf16[32,2,3,2048]{3,1,2,0:T(2,128)(2,1)S(1)}, u32[]{:S(2)}, u32[]{:S(2)}) async-start(bf16[32,2,3,2048]{3,1,2,0:T(2,128)(2,1)} %copy.75), calls=%async_computation.4 | async-start | bytes 1572864 | tf_op jit(solution)/shard_map/all_to_all | solution.py:117
  152.0 46.0 %all-gather.6.cloned.1.call-start = ((), (), s32[]{:S(2)}) async-start(), calls=%async_computation.7 | async-start | bytes 1769472 | tf_op jit(solution)/shard_map/all_gather | solution.py:120
  152.2 45.8 %copy-start.3 = (bf16[2048,64]{0,1:T(8,128)(2,1)S(1)}, bf16[2048,64]{0,1:T(8,128)(2,1)}, u32[]{:S(2)}) copy-start(bf16[2048,64]{0,1:T(8,128)(2,1)} %param.31) | copy-start | bytes 786436
  153.0 125.6 %all-gather.4.cloned.1.call-start = ((), (), s32[]{:S(2)}) async-start(), calls=%async_computation.6 | async-start | bytes 7077888 | tf_op jit(solution)/shard_map/all_gather | solution.py:119
  197.7 130.9 %all-gather.8.cloned.1.call-start = ((), (), s32[]{:S(2)}) async-start(), calls=%async_computation.8 | async-start | bytes 2211840 | tf_op jit(solution)/shard_map/all_gather | solution.py:42
  198.0 2.1 copy-start.2
  200.2 78.4 %copy-start.10 = (bf16[2,2048,64]{1,2,0:T(8,128)(2,1)S(1)}, bf16[2,2048,64]{1,2,0:T(8,128)(2,1)}, u32[]{:S(2)}) copy-start(bf16[2,2048,64]{1,2,0:T(8,128)(2,1)} %param.28) | copy-start | bytes 1572868
  201.9 81.4 %copy-start.11 = (bf16[2,2048,64]{1,2,0:T(8,128)(2,1)S(1)}, bf16[2,2048,64]{1,2,0:T(8,128)(2,1)}, u32[]{:S(2)}) copy-start(bf16[2,2048,64]{1,2,0:T(8,128)(2,1)} %param.29) | copy-start | bytes 1572868
  278.6 4.7 %copy-start.9 = (bf16[32,2,24,2048]{3,0,1,2:T(8,128)(2,1)S(1)}, bf16[32,2,24,2048]{3,0,1,2:T(8,128)(2,1)}, u32[]{:S(2)}) copy-start(bf16[32,2,24,2048]{3,0,1,2:T(8,128)(2,1)} %all-gather.4.cloned.1.call-done) | copy-start | bytes 18874372
  328.6 1.4 slice-start
  333.7 19.0 %copy-start.6 = (f32[384,2]{0,1:T(2,128)S(1)}, f32[384,2]{0,1:T(2,128)}, u32[]{:S(2)}) copy-start(f32[384,2]{0,1:T(2,128)} %param.27) | copy-start | bytes 9220
  334.7 62.5 %all-to-all-start.5 = ((bf16[32,2,24,256]{3,2,1,0:T(8,128)(2,1)}), bf16[32,2,24,256]{3,2,1,0:T(8,128)(2,1)S(1)}, u32[]{:S(2)}, u32[]{:S(2)}) async-start(bf16[32,2,24,256]{3,2,1,0:T(8,128)(2,1)} %copy.85), calls=%async_computation.5 | async-start | bytes 1572864 | tf_op jit(solution)/shard_map/all_to_all | solution.py:140
  400.4 3.5 copy-start.1
Sparse Core Ops, SparseCore 0:
  154.9 37.8 all-gather.5
  197.8 80.6 all-gather.3
  286.5 42.1 all-gather.7
where the time goes:
time: 413 us; the launch traced here: 412 us
  waiting for transfers between devices  287 us (69%)
  starting transfers between devices  54 us (13%)
  local copies, waits for them, and re-layouts  23.7 us (6%)
  matrix products  14.9 us (4%)
  between operations  13.6 us (3%)
  other arithmetic  9.74 us (2%)
  blocking collectives  9.06 us (2%)
    all_gather x1, waiting for transfers between devices, body(): lax.all_gather(got, 'tp', axis=2, tiled=True)  76.6 us
    all_to_all x1, waiting for transfers between devices, body(): lax.all_to_all(expert_part.astype(jnp.bfloat16), 'sp', split_axis=0, conc...  43.6 us
    all_to_all x1, waiting for transfers between devices, body(): lax.all_to_all(padded_block[local], 'sp', split_axis=0, concat_axis=0, ti...  43.3 us
    all_gather x1, waiting for transfers between devices, rows_first(): lax.all_gather(both, axis, axis=0, tiled=True)  42.3 us
    all_to_all x1, waiting for transfers between devices, sum_at_owner(): lax.all_to_all(pieces, axis, split_axis=0, concat_axis=0, tiled=True)  35.1 us
    ppermute x2, waiting for transfers between devices, from_behind(): lax.ppermute(value, axis, [(source, source + steps) for source in range(f...  34.9 us
    all_to_all x1, starting transfers between devices, body(): lax.all_to_all(expert_part.astype(jnp.bfloat16), 'sp', split_axis=0, conc...  18.1 us
    all_to_all x1, starting transfers between devices, body(): lax.all_to_all(padded_block[local], 'sp', split_axis=0, concat_axis=0, ti...  15.3 us
  transfers between devices with their start and end apart: 10, of which 8 were waited for; matrix products, arithmetic and copies ran while one was open for 4% of the time, Pallas kernels for 0%

commit v1 on v0

--- a/solution.py
+++ b/solution.py
@@ -116,7 +116,7 @@
     padded_block = jnp.concatenate([block_rows, jnp.zeros((1, width), jnp.bfloat16)], axis=0)
     got = lax.all_to_all(padded_block[local], "sp", split_axis=0, concat_axis=0, tiled=True)
     arrived, whole = (
-        lax.all_gather(got, "tp", axis=2, tiled=True),
+        jnp.concatenate(lax.all_to_all(jnp.stack([got] * lax.axis_size("tp")), "tp", 0, 0), axis=2),
         lax.all_gather(block_rows.reshape(1, 1, rows, width), "tp", axis=2, tiled=True),
     )
     normal = whole.reshape(tokens, width)

time: 413 us -> 484 us (1.17)
  blocking collectives: 9.06 us -> 68.6 us
  waiting for transfers between devices: 287 us -> 307 us
  starting transfers between devices: 54 us -> 43.7 us
  local copies, waits for them, and re-layouts: 23.7 us -> 28.7 us
    all_gather x1 -> x0, waiting for transfers between devices: 76.6 us -> none  [body(): lax.all_gather(got, 'tp', axis=2, tiled=True)]
    all_gather x1, waiting for transfers between devices: 0.02 us -> 75.1 us  [body(): lax.all_gather(block_rows.reshape(1, 1, rows, width), 'tp', axis=2, tiled...]
    all_to_all x0 -> x1, blocking collectives: none -> 59.5 us  [body(): lax.all_to_all(padded_block[local], 'sp', split_axis=0, concat_axis=0, ti...]
    all_to_all x1, waiting for transfers between devices: 43.3 us -> 77.1 us  [body(): lax.all_to_all(jnp.stack([got] * lax.axis_size('tp')), 'tp', 0, 0)]
    all_gather x1, waiting for transfers between devices: 42.3 us -> 30 us  [rows_first(): lax.all_gather(both, axis, axis=0, tiled=True)]
    all_to_all x1, starting transfers between devices: 15.3 us -> 5.06 us  [body(): lax.all_to_all(jnp.stack([got] * lax.axis_size('tp')), 'tp', 0, 0)]
  transfers between devices with their start and end apart: 10 -> 9, of which waited for: 8 -> 8; matrix products, arithmetic and copies ran while one was open for 4% -> 3% of each run, Pallas kernels for 0% -> 0%
where the time goes in v1:
time: 484 us; the launch traced here: 483 us
  waiting for transfers between devices  307 us (63%)
  blocking collectives  68.6 us (14%)
  starting transfers between devices  43.7 us (9%)
  local copies, waits for them, and re-layouts  28.7 us (6%)
  between operations  13.9 us (3%)
  matrix products  10.8 us (2%)
  other arithmetic  9.74 us (2%)
    all_to_all x1, waiting for transfers between devices, body(): lax.all_to_all(jnp.stack([got] * lax.axis_size('tp')), 'tp', 0, 0)  77.1 us
    all_gather x1, waiting for transfers between devices, body(): lax.all_gather(block_rows.reshape(1, 1, rows, width), 'tp', axis=2, tiled...  75.1 us
    all_to_all x1, blocking collectives, body(): lax.all_to_all(padded_block[local], 'sp', split_axis=0, concat_axis=0, ti...  59.5 us
    all_to_all x1, waiting for transfers between devices, body(): lax.all_to_all(expert_part.astype(jnp.bfloat16), 'sp', split_axis=0, conc...  43.6 us
    all_to_all x1, waiting for transfers between devices, sum_at_owner(): lax.all_to_all(pieces, axis, split_axis=0, concat_axis=0, tiled=True)  35.1 us
    ppermute x2, waiting for transfers between devices, from_behind(): lax.ppermute(value, axis, [(source, source + steps) for source in range(f...  34.9 us
    all_gather x1, waiting for transfers between devices, rows_first(): lax.all_gather(both, axis, axis=0, tiled=True)  30 us
    all_to_all x1, starting transfers between devices, body(): lax.all_to_all(expert_part.astype(jnp.bfloat16), 'sp', split_axis=0, conc...  18.1 us
  transfers between devices with their start and end apart: 9, of which 8 were waited for; matrix products, arithmetic and copies ran while one was open for 3% of the time, Pallas kernels for 0%

profile of v1, /device:TPU:65, one launch (start us, length us, event | category | flops | bytes accessed | tf_op | source)
XLA Modules:
  0.0 482.7 jit_solution(10616251995891030938)
XLA Ops:
  7.6 7.1 %collective-permute-start.1 = (bf16[2,128]{1,0:T(2,128)(2,1)S(1)}, bf16[2,128]{1,0:T(2,128)(2,1)S(1)}, u32[]{:S(2)}, u32[]{:S(2)}) collective-permute-start(bf16[2,128]{1,0:T(2,128)(2,1)S(1)} %slice.53), channel_id=1, source_target_pairs={{0,8},{8,16},{16,24},{24,32},{32,40},{40,48},{48,56},{56,64},{64,7... | collective-permute-start | bytes 1544 | tf_op jit(solution)/shard_map/ppermute | solution.py:15
  15.4 1.9 collective-permute-start
  18.2 34.9 %collective-permute-done = bf16[2]{0:T(256)(128)(2,1)S(1)} collective-permute-done((bf16[2]{0:T(256)(128)(2,1)S(1)}, bf16[2]{0:T(256)(128)(2,1)S(1)}, u32[]{:S(2)}, u32[]{:S(2)}) %collective-permute-start) | collective-permute-done | bytes 36 | tf_op jit(solution)/shard_map/ppermute | solution.py:15
  55.8 9.1 %all_to_all.51 = f32[8,1,384]{2,1,0:T(1,128)S(1)} all-to-all(f32[8,1,384]{2,1,0:T(1,128)S(1)} %broadcast_in_dim.50), channel_id=1, replica_groups=mesh['grp'=2,'sp'=32,'tp'=8] {'tp'}, dimensions={0} | all-to-all | bytes 24576 | tf_op jit(solution)/shard_map/all_to_all | solution.py:20
  65.5 1.3 copy.102
  66.7 3.9 all-to-all-start.1
  71.1 1.9 select_reduce_fusion
  73.5 35.1 %all-to-all-done.1 = bf16[8,384,256]{2,1,0:T(8,128)(2,1)S(1)} async-done(((bf16[8,384,256]{2,1,0:T(8,128)(2,1)}), bf16[8,384,256]{2,1,0:T(8,128)(2,1)S(1)}, u32[]{:S(2)}, u32[]{:S(2)}) %all-to-all-start.1) | async-done | bytes 1572896 | tf_op jit(solution)/shard_map/all_to_all | solution.py:35
  109.6 3.7 all-to-all-start.2
  113.3 3.4 scatter_custom_fusion
  116.9 3.0 all-to-all-done.2
  120.8 3.7 all-to-all-start.3
  124.7 8.5 %all-to-all-done.3 = bf16[8,48,256]{2,1,0:T(8,128)(2,1)S(1)} async-done(((bf16[8,48,256]{2,1,0:T(8,128)(2,1)}), bf16[8,48,256]{2,1,0:T(8,128)(2,1)S(1)}, u32[]{:S(2)}, u32[]{:S(2)}) %all-to-all-start.3) | async-done | bytes 196640 | tf_op jit(solution)/shard_map/all_to_all | solution.py:111
  135.8 59.5 %all_to_all.52 = bf16[32,2,3,2048]{3,1,2,0:T(2,128)(2,1)S(1)} all-to-all(bf16[32,2,3,2048]{3,1,2,0:T(2,128)(2,1)S(1)} %copy.76), channel_id=1, replica_groups=mesh['grp'=2,'sp'=32,'tp'=8] {'sp'}, dimensions={0} | all-to-all | bytes 1572864 | tf_op jit(solution)/shard_map/all_to_all | solution.py:117
  195.6 3.5 stack.2
  199.1 5.1 %all-to-all-start.5 = ((bf16[8,32,2,3,2048]{4,1,3,2,0:T(8,128)(2,1)}), bf16[8,32,2,3,2048]{4,1,3,2,0:T(8,128)(2,1)}, u32[]{:S(2)}, u32[]{:S(2)}) async-start(bf16[8,32,2,3,2048]{4,1,3,2,0:T(8,128)(2,1)} %stack.2), calls=%async_computation.5 | async-start | bytes 12582912 | tf_op jit(solution)/shard_map/all_to_all | solution.py:119
  205.4 75.1 %all-gather.3.cloned.1.call-done = bf16[1,1,384,2048]{3,2,1,0:T(8,128)(2,1)} async-done(((bf16[1,1,48,2048]{3,2,1,0:T(8,128)(2,1)}), bf16[1,1,384,2048]{3,2,1,0:T(8,128)(2,1)}) %all-gather.3.cloned.1.call-update) | async-done | bytes 1572880 | tf_op jit(solution)/shard_map/all_gather | solution.py:120
  280.4 2.1 fusion.16
  283.3 77.1 %all-to-all-done.5 = bf16[8,32,2,3,2048]{4,1,3,2,0:T(8,128)(2,1)} async-done(((bf16[8,32,2,3,2048]{4,1,3,2,0:T(8,128)(2,1)}), bf16[8,32,2,3,2048]{4,1,3,2,0:T(8,128)(2,1)}, u32[]{:S(2)}, u32[]{:S(2)}) %all-to-all-start.5) | async-done | bytes 6291488 | tf_op jit(solution)/shard_map/all_to_all | solution.py:119
  360.5 3.4 copy.78
  363.9 1.8 convolution_bitcast_fusion.1
  365.6 1.8 fusion.13
  368.7 30.0 %all-gather.5.cloned.1.call-done = bf16[512,1920]{1,0:T(8,128)(2,1)} async-done(((bf16[64,1920]{1,0:T(8,128)(2,1)}), bf16[512,1920]{1,0:T(8,128)(2,1)}) %all-gather.5.cloned.1.call-update) | async-done | bytes 1966096 | tf_op jit(solution)/shard_map/all_gather | solution.py:42
  398.7 1.4 slice-done
  400.1 1.6 copy.92
  401.7 2.0 fusion.9
  404.7 18.1 %all-to-all-start.6 = ((bf16[32,2,24,256]{3,2,1,0:T(8,128)(2,1)}), bf16[32,2,24,256]{3,2,1,0:T(8,128)(2,1)S(1)}, u32[]{:S(2)}, u32[]{:S(2)}) async-start(bf16[32,2,24,256]{3,2,1,0:T(8,128)(2,1)} %copy.85), calls=%async_computation.6 | async-start | bytes 1572864 | tf_op jit(solution)/shard_map/all_to_all | solution.py:140
  423.6 43.6 %all-to-all-done.6 = bf16[32,2,24,256]{3,2,1,0:T(8,128)(2,1)S(1)} async-done(((bf16[32,2,24,256]{3,2,1,0:T(8,128)(2,1)}), bf16[32,2,24,256]{3,2,1,0:T(8,128)(2,1)S(1)}, u32[]{:S(2)}, u32[]{:S(2)}) %all-to-all-start.6) | async-done | bytes 786464 | tf_op jit(solution)/shard_map/all_to_all | solution.py:140
  467.1 3.3 gather_fusion.1
  470.4 1.5 reshape.197
  471.9 2.0 multiply_reduce_fusion
  473.9 1.9 fusion.15
  (83 shorter events, 17.0 us)
Async XLA Ops:
  6.5 58.3 %copy-start = (bf16[128,2048]{1,0:T(8,128)(2,1)S(1)}, bf16[128,2048]{1,0:T(8,128)(2,1)}, u32[]{:S(2)}) copy-start(bf16[128,2048]{1,0:T(8,128)(2,1)} %param.24) | copy-start | bytes 1572868
  6.6 58.3 %copy-start.9 = (f32[128]{0:T(128)S(1)}, f32[128]{0:T(128)}, u32[]{:S(2)}) copy-start(f32[128]{0:T(128)} %param.23) | copy-start | bytes 1540
  7.6 47.0 %collective-permute-start.1 = (bf16[2,128]{1,0:T(2,128)(2,1)S(1)}, bf16[2,128]{1,0:T(2,128)(2,1)S(1)}, u32[]{:S(2)}, u32[]{:S(2)}) collective-permute-start(bf16[2,128]{1,0:T(2,128)(2,1)S(1)} %slice.53), channel_id=1, source_target_pairs={{0,8},{8,16},{16,24},{24,32},{32,40},{40,48},{48,56},{56,64},{64,7... | collective-permute-start | bytes 1544 | tf_op jit(solution)/shard_map/ppermute | solution.py:15
  15.4 37.6 %collective-permute-start = (bf16[2]{0:T(256)(128)(2,1)S(1)}, bf16[2]{0:T(256)(128)(2,1)S(1)}, u32[]{:S(2)}, u32[]{:S(2)}) collective-permute-start(bf16[2]{0:T(256)(128)(2,1)S(1)} %slice.37), channel_id=1, source_target_pairs={{0,8},{8,16},{16,24},{24,32},{32,40},{40,48},{48,56},{56,64},{64,7... | collective-permute-start | bytes 20 | tf_op jit(solution)/shard_map/ppermute | solution.py:15
  66.7 3.9 copy-start.6
  66.7 41.9 %all-to-all-start.1 = ((bf16[8,384,256]{2,1,0:T(8,128)(2,1)}), bf16[8,384,256]{2,1,0:T(8,128)(2,1)S(1)}, u32[]{:S(2)}, u32[]{:S(2)}) async-start(bf16[8,384,256]{2,1,0:T(8,128)(2,1)} %bitcast.81), calls=%async_computation.1 | async-start | bytes 3145728 | tf_op jit(solution)/shard_map/all_to_all | solution.py:35
  70.7 38.2 %copy-start.5 = (bf16[384,256]{1,0:T(8,128)(2,1)S(1)}, bf16[384,256]{1,0:T(8,128)(2,1)}, u32[]{:S(2)}) copy-start(bf16[384,256]{1,0:T(8,128)(2,1)} %param.21) | copy-start | bytes 589828
  73.5 46.5 %copy-start.8 = (f32[256]{0:T(256)S(1)}, f32[256]{0:T(256)}, u32[]{:S(2)}) copy-start(f32[256]{0:T(256)} %param.25) | copy-start | bytes 3076
  109.6 10.3 %all-to-all-start.2 = ((f32[8,1,384]{2,1,0:T(1,128)}), f32[8,1,384]{2,1,0:T(1,128)S(1)}, u32[]{:S(2)}, u32[]{:S(2)}) async-start(f32[8,1,384]{2,1,0:T(1,128)} %broadcast_in_dim.51), calls=%async_computation.2 | async-start | bytes 24576 | tf_op jit(solution)/shard_map/all_to_all | solution.py:20
  120.8 12.4 %all-to-all-start.3 = ((bf16[8,48,256]{2,1,0:T(8,128)(2,1)}), bf16[8,48,256]{2,1,0:T(8,128)(2,1)S(1)}, u32[]{:S(2)}, u32[]{:S(2)}) async-start(bf16[8,48,256]{2,1,0:T(8,128)(2,1)} %bitcast.4), calls=%async_computation.3 | async-start | bytes 393216 | tf_op jit(solution)/shard_map/all_to_all | solution.py:111
  199.1 81.4 %copy-start.4 = (bf16[2048,64]{0,1:T(8,128)(2,1)S(1)}, bf16[2048,64]{0,1:T(8,128)(2,1)}, u32[]{:S(2)}) copy-start(bf16[2048,64]{0,1:T(8,128)(2,1)} %param.31) | copy-start | bytes 786436
  199.1 161.4 %all-to-all-start.5 = ((bf16[8,32,2,3,2048]{4,1,3,2,0:T(8,128)(2,1)}), bf16[8,32,2,3,2048]{4,1,3,2,0:T(8,128)(2,1)}, u32[]{:S(2)}, u32[]{:S(2)}) async-start(bf16[8,32,2,3,2048]{4,1,3,2,0:T(8,128)(2,1)} %stack.2), calls=%async_computation.5 | async-start | bytes 12582912 | tf_op jit(solution)/shard_map/all_to_all | solution.py:119
  204.1 78.5 %copy-start.12 = (bf16[2048,64]{0,1:T(8,128)(2,1)S(1)}, bf16[2048,64]{0,1:T(8,128)(2,1)}, u32[]{:S(2)}) copy-start(bf16[2048,64]{0,1:T(8,128)(2,1)} %param.32) | copy-start | bytes 786436
  204.1 76.3 %all-gather.3.cloned.1.call-start = ((), (), s32[]{:S(2)}) async-start(), calls=%async_computation.7 | async-start | bytes 1769472 | tf_op jit(solution)/shard_map/all_gather | solution.py:120
  205.1 193.6 %all-gather.5.cloned.1.call-start = ((), (), s32[]{:S(2)}) async-start(), calls=%async_computation.8 | async-start | bytes 2211840 | tf_op jit(solution)/shard_map/all_gather | solution.py:42
  280.4 2.1 copy-start.2
  283.3 80.5 %copy-start.3 = (bf16[2,2048,64]{1,2,0:T(8,128)(2,1)S(1)}, bf16[2,2048,64]{1,2,0:T(8,128)(2,1)}, u32[]{:S(2)}) copy-start(bf16[2,2048,64]{1,2,0:T(8,128)(2,1)} %param.28) | copy-start | bytes 1572868
  363.8 1.8 copy-start.10
  398.7 1.4 slice-start
  400.1 1.6 copy-start.11
  403.7 19.1 %copy-start.7 = (f32[384,2]{0,1:T(2,128)S(1)}, f32[384,2]{0,1:T(2,128)}, u32[]{:S(2)}) copy-start(f32[384,2]{0,1:T(2,128)} %param.27) | copy-start | bytes 9220
  404.7 62.5 %all-to-all-start.6 = ((bf16[32,2,24,256]{3,2,1,0:T(8,128)(2,1)}), bf16[32,2,24,256]{3,2,1,0:T(8,128)(2,1)S(1)}, u32[]{:S(2)}, u32[]{:S(2)}) async-start(bf16[32,2,24,256]{3,2,1,0:T(8,128)(2,1)} %copy.85), calls=%async_computation.6 | async-start | bytes 1572864 | tf_op jit(solution)/shard_map/all_to_all | solution.py:140
  470.4 3.5 copy-start.1
Sparse Core Ops, SparseCore 0:
  207.1 73.3 all-gather.2
  368.8 29.8 all-gather.4
